TPU v7x, 32 devices: a whole 2x2x4 slice. The times are simulated.
32 devices in a mesh: gr: 2 (over x), sp: 8 (over z, y), tp: 2 (over core).
Axes of the slice: x: 2, y: 2, z: 4, core: 2. Of those that a mesh axis runs over, the one named last changes fastest.
Arguments:
- inputs: bfloat16 [4096, 2048], P(('gr', 'sp'), 'tp'), parts along dimension 0, may hold values from -6 to 6
- x_weight: bfloat16 [2048, 4096], P(None, 'tp'), may hold values from -0.125 to 0.125
- b_weight: bfloat16 [2048, 2048], P(None, 'tp'), may hold values from -0.125 to 0.125
- dt_weight: bfloat16 [2048, 128], replicated, may hold values from -0.125 to 0.125
- dt_bias: float32 [2, 64], replicated, may hold values from -2 to -1
- decay_rate: float32 [2, 64], replicated, may hold values from 0.3 to 10
- conv_x: bfloat16 [5, 4096], P(None, 'tp'), may hold values from -2.5 to 2.5
- conv_b: bfloat16 [5, 2048], P(None, 'tp'), may hold values from -2.5 to 2.5
- query_c: bfloat16 [2, 16, 128], P('gr', 'tp'), parts along dimension 0, may hold values from -6 to 6
- query_gate: bfloat16 [2, 64, 64], P('gr', 'tp'), parts along dimension 0, may hold values from -6 to 6
- read_span: int32 [2], P('gr'), parts along dimension 0, may hold values from 0 to 15
- read_gain: float32 [64, 64], P('tp'), may hold values from 0.1 to 1.9
Outputs:
- span_cache: bfloat16 [32, 2, 64, 8192], P('gr', None, 'tp', 'sp'), parts along dimension 0
- first_read: bfloat16 [2, 64, 64], P('gr', 'tp'), parts along dimension 0
There are 2 independent parts, one for each index of `gr`. A program takes and returns all parts, laid end to end along the dimension named above; an argument that names none is the same for every part. Nothing has to cross between parts.
Inputs may be any that keep to these rules, and one draw needn't show every extreme that they name: read_span holds one span index from 0 to 15.
All inputs are finite; a program needn't handle non-finite values.
Results may differ from a plain program's by a relative error of at most 0.009.
Values may be sent and summed in bfloat16 or wider, within the bound.
A program may use at most 64 MiB of HBM per device.

v0:
```python
import jax
import jax.numpy as jnp
from jax import lax
from jax.sharding import PartitionSpec as P

H = 64
P_SIZE = 64
G = 16
N = 128
KW = 5
SPAN = 128
EPSILON = 1e-06


def extended(shard, sides, width):
    for axis, dim in sides:
        size, length = (lax.axis_size(axis), shard.shape[dim])
        up = [(i, (i + 1) % size) for i in range(size - 1)]
        down = [(j, i) for i, j in up]
        last = lax.slice_in_dim(shard, length - width, length, axis=dim)
        initial = lax.slice_in_dim(shard, 0, width, axis=dim)
        before = lax.ppermute(last, axis, up)
        after = lax.ppermute(initial, axis, down)
        shard = jnp.concatenate([before, shard, after], axis=dim)
    return shard


def span_states(value_rows, key_rows, step_sizes, log_decay):
    running = jnp.cumsum(log_decay, axis=1)
    closing = running[:, -1]
    forward = jnp.exp(closing[:, None, 0] - running[:, :, 0]) * step_sizes[:, :, 0]
    backward = jnp.exp(running[:, :, 1] - log_decay[:, :, 1]) * step_sizes[:, :, 1]
    weights = jnp.stack([forward, backward], axis=2)
    states = jnp.einsum(
        "kseh,kshn,kshp->kehnp",
        weights,
        key_rows.astype(jnp.float32),
        value_rows.astype(jnp.float32),
    )
    return (states, closing)


def read_weights(span_logs, chosen):
    span_count = span_logs.shape[0]
    ahead_sum = jnp.cumsum(span_logs[:, 0], axis=0)
    behind = jnp.flip(jnp.cumsum(jnp.flip(span_logs[:, 1], 0), axis=0), 0)
    positions = jnp.arange(span_count, dtype=jnp.int32)[:, None]
    ahead_pick = lax.dynamic_slice_in_dim(ahead_sum, chosen, 1, 0)
    behind_pick = lax.dynamic_slice_in_dim(behind, chosen, 1, 0)
    before = positions <= chosen
    after = positions >= chosen
    forward = jnp.where(before, jnp.exp(jnp.where(before, ahead_pick - ahead_sum, 0.0)), 0.0)
    backward = jnp.where(after, jnp.exp(jnp.where(after, behind_pick - behind, 0.0)), 0.0)
    return jnp.stack([forward, backward], axis=1)


def per_device(
    inputs,
    x_weight,
    b_weight,
    dt_weight,
    dt_bias,
    decay_rate,
    conv_x,
    conv_b,
    query_c,
    query_gate,
    read_span,
    read_gain,
):
    tokens = inputs.shape[0]
    heads_local = x_weight.shape[1] // P_SIZE
    per_group = H // G
    tp_index = lax.axis_index("tp")
    sp_index = lax.axis_index("sp")
    dt_local = lax.dynamic_slice_in_dim(
        dt_weight.reshape(dt_weight.shape[0], 2, H), tp_index * heads_local, heads_local, 2
    )
    dt_local = dt_local.reshape(dt_weight.shape[0], 2 * heads_local)
    slab_piece = lax.all_gather(inputs, "tp", axis=1, tiled=True)
    x_part = jnp.dot(slab_piece, x_weight, preferred_element_type=jnp.float32)
    b_part = jnp.dot(slab_piece, b_weight, preferred_element_type=jnp.float32)
    dt_part = jnp.dot(slab_piece, dt_local, preferred_element_type=jnp.float32)
    joined = jnp.concatenate([x_part.astype(jnp.bfloat16), b_part.astype(jnp.bfloat16)], axis=1)
    reach = KW // 2
    padded = extended(joined, (("sp", 0),), reach)
    taps = jnp.concatenate([conv_x, conv_b], axis=1)
    mixed_rows = jnp.zeros(joined.shape, jnp.float32)
    for offset in range(KW):
        mixed_rows = mixed_rows + taps[offset].astype(jnp.float32) * padded[
            offset : offset + tokens
        ].astype(jnp.float32)
    mixed_rows = jax.nn.silu(mixed_rows).astype(jnp.bfloat16)
    split_at = x_weight.shape[1]
    values = mixed_rows[:, :split_at]
    key_rows = mixed_rows[:, split_at:]
    length = tokens * lax.axis_size("sp")
    bias_local = lax.dynamic_slice_in_dim(dt_bias, tp_index * heads_local, heads_local, 1)
    rate_local = lax.dynamic_slice_in_dim(decay_rate, tp_index * heads_local, heads_local, 1)
    dt_raw = dt_part.astype(jnp.bfloat16).reshape(tokens, 2, heads_local)
    step_sizes = jax.nn.softplus(dt_raw.astype(jnp.float32) + bias_local)
    log_decay = -(step_sizes * rate_local) / length
    span_count = tokens // SPAN
    value_rows = values.reshape(span_count, SPAN, heads_local, P_SIZE)
    group_keys = key_rows.reshape(span_count, SPAN, heads_local // per_group, N)
    group_keys = jnp.repeat(group_keys, per_group, axis=2)
    states, closing = span_states(
        value_rows,
        group_keys,
        step_sizes.reshape(span_count, SPAN, 2, heads_local),
        log_decay.reshape(span_count, SPAN, 2, heads_local),
    )
    local_rows = states.reshape(span_count, 2, heads_local, N * P_SIZE).astype(jnp.bfloat16)
    all_logs = lax.all_gather(closing, "sp", axis=0, tiled=True)
    weights = read_weights(all_logs, read_span[0])
    cache_rows = lax.all_to_all(local_rows, "sp", split_axis=3, concat_axis=0, tiled=True)
    columns = cache_rows.shape[3] // P_SIZE
    gathered = jnp.einsum("jeh,jehx->hx", weights, cache_rows.astype(jnp.float32)).reshape(
        heads_local, columns, P_SIZE
    )
    picked = lax.dynamic_slice_in_dim(query_c[0], sp_index * columns, columns, 1)
    query_cols = jnp.repeat(picked.astype(jnp.float32), per_group, axis=0)
    partial_read = jnp.einsum("hnp,hn->hp", gathered, query_cols)
    read_total = lax.psum(partial_read, "sp")
    gated_read = read_total * jax.nn.silu(query_gate[0].astype(jnp.float32))
    square_sum = lax.psum(jnp.sum(gated_read * gated_read), "tp")
    mean_square = square_sum / (H * P_SIZE)
    first_read = (gated_read * lax.rsqrt(mean_square + EPSILON) * read_gain)[None].astype(
        jnp.bfloat16
    )
    return (cache_rows, first_read)


def solution(mesh):
    return jax.shard_map(
        per_device,
        mesh=mesh,
        in_specs=(
            P(("gr", "sp"), "tp"),
            P(None, "tp"),
            P(None, "tp"),
            P(),
            P(),
            P(),
            P(None, "tp"),
            P(None, "tp"),
            P("gr", "tp", None),
            P("gr", "tp", None),
            P("gr"),
            P("tp", None),
        ),
        out_specs=(P("gr", None, "tp", "sp"), P("gr", "tp", None)),
        check_vma=False,
    )
```

profile of v0, /device:TPU:0, one launch (start us, length us, event | category | flops | bytes accessed | tf_op | source)
XLA Modules:
  0.0 222.9 jit_solution(17773302501208012883)
XLA Ops:
  7.9 0.8 constant_dynamic-update-slice_fusion.1
  8.7 0.8 constant_dynamic-slice_fusion.2
  9.4 1.2 copy.63
  10.7 0.7 constant_dynamic-update-slice_fusion
  11.5 9.8 %all-gather.3.cloned.1.call-done = bf16[256,2048]{1,0:T(8,128)(2,1)} async-done(((bf16[256,1024]{1,0:T(8,128)(2,1)}), bf16[256,2048]{1,0:T(8,128)(2,1)}) %all-gather.3.cloned.1.call-update) | async-done | bytes 1048592 | tf_op jit(solution)/shard_map/all_gather | solution.py:80
  21.3 1.8 fusion.9
  23.9 5.9 %convolution_convert_fusion = bf16[256,2048]{1,0:T(8,128)(2,1)S(1)} fusion(bf16[256,2048]{1,0:T(8,128)(2,1)S(1)} %copy-done.1, bf16[2048,2048]{1,0:T(8,128)(2,1)} %param.13), kind=kOutput, calls=%fused_computation.3 | convolution fusion | flops 2148007936 | bytes 10485760 | tf_op jit(solution)/shard_map/dot_general | solution.py:81
  29.8 1.3 convolution_convert_fusion.1
  31.1 3.6 %collective-permute-start = (bf16[2,3072]{1,0:T(2,128)(2,1)S(1)}, bf16[2,3072]{1,0:T(2,128)(2,1)S(1)}, u32[]{:S(2)}, u32[]{:S(2)}) collective-permute-start(bf16[2,3072]{1,0:T(2,128)(2,1)S(1)} %get-tuple-element.6), channel_id=1, source_target_pairs={{0,2},{2,4},{4,6},{6,8},{8,10},{10,12},{12,14},{1,3},{3,5},{5,7},{... | collective-permute-start | bytes 36872 | tf_op jit(solution)/shard_map/ppermute | solution.py:22
  34.8 1.3 collective-permute-start.1
  36.3 4.1 %collective-permute-done.1 = bf16[2,3072]{1,0:T(2,128)(2,1)S(1)} collective-permute-done((bf16[2,3072]{1,0:T(2,128)(2,1)S(1)}, bf16[2,3072]{1,0:T(2,128)(2,1)S(1)}, u32[]{:S(2)}, u32[]{:S(2)}) %collective-permute-start.1) | collective-permute-done | bytes 12320 | tf_op jit(solution)/shard_map/ppermute | solution.py:23
  40.9 2.9 %multiply_convert_fusion = bf16[256,3072]{1,0:T(8,128)(2,1)S(1)} fusion(bf16[256,1024]{1,0:T(8,128)(2,1)S(1)} %convolution_convert_fusion.1, bf16[256,2048]{1,0:T(8,128)(2,1)S(1)} %convolution_convert_fusion, bf16[258,3072]{1,0:T(8,128)(2,1)S(1)} %get-tuple-element.5, bf16[258,3072]{1,0:T(8,128)(2,1)S(1)} %get-tuple-element.4, f32[3072]{0:T(1024)S(1)} %bitcast.103, ...), kind=kLoop, calls=%fused_computation.2 | loop fusion | flops 17301504 | bytes 9498624 | tf_op jit(solution)/shard_map/convert_element_type | solution.py:93
  44.0 3.0 %reshape.152 = f32[2,128,32,64]{3,2,1,0:T(8,128)} reshape(f32[256,2048]{1,0:T(8,128)S(1)} %slice_convert_fusion) | data formatting | bytes 4194304 | tf_op jit(solution)/shard_map/convert.7
  47.0 3.8 %copy.62 = f32[2,128,32,64]{1,3,2,0:T(8,128)S(1)} copy(f32[2,128,32,64]{3,2,1,0:T(8,128)} %reshape.152) | data formatting | bytes 4194304 | tf_op jit(solution)/shard_map/convert.7
  51.6 2.0 convert_bitcast_fusion
  53.6 14.1 %copy.82 = bf16[2,2,32,128,64]{2,1,0,4,3:T(2,128)(2,1)} copy(bf16[2,2,32,128,64]{3,4,1,2,0:T(8,128)(2,1)} %convert_bitcast_fusion) | data formatting | bytes 4194304 | tf_op jit(solution)/shard_map/convert_element_type | solution.py:113
  67.7 11.2 %reshape.153 = bf16[8,2,65536]{2,1,0:T(2,128)(2,1)} reshape(bf16[8192,2,2,32]{3,2,1,0:T(2,128)(2,1)} %bitcast.92) | data formatting | bytes 4194304
  78.9 5.6 %all-to-all-start = ((bf16[8,2,65536]{2,1,0:T(2,128)(2,1)}), bf16[8,2,65536]{2,1,0:T(2,128)(2,1)S(1)}, u32[]{:S(2)}, u32[]{:S(2)}) async-start(bf16[8,2,65536]{2,1,0:T(2,128)(2,1)} %reshape.153), calls=%async_computation | async-start | bytes 4194304 | tf_op jit(solution)/shard_map/all_to_all | solution.py:116
  85.2 65.2 %all-gather = f32[16,1,2,32]{3,2,1,0:T(2,128)S(1)} all-gather(f32[2,1,2,32]{3,2,1,0:T(2,128)S(1)} %get-tuple-element.8), channel_id=2, replica_groups=mesh['gr'=2,'sp'=8,'tp'=2] {'sp'}, dimensions={0}, use_global_device_ids=true | all-gather | bytes 4608 | tf_op jit(solution)/shard_map/all_gather | solution.py:114
  150.8 6.6 %reshape.154 = bf16[8192,2,2,32]{3,2,1,0:T(2,128)(2,1)} reshape(bf16[8,2,65536]{2,1,0:T(2,128)(2,1)S(1)} %all-to-all-done) | data formatting | bytes 4194304
  157.4 17.8 %copy.84 = bf16[2,2,32,8,1024]{4,2,1,0,3:T(8,128)(2,1)S(1)} copy(bf16[2,2,32,8,1024]{2,1,0,4,3:T(2,128)(2,1)} %bitcast.93) | data formatting | bytes 4194304 | tf_op jit(solution)/shard_map/all_to_all | solution.py:116
  175.2 2.4 %fusion.2 = bf16[32,1,1024,1]{2,1,3,0:T(2,128)(2,1)S(1)} fusion(bf16[16,2,32,1]{0,3,1,2:T(2,128)(2,1)S(1)} %copy.75, bf16[16,2,32,1024]{3,2,1,0:T(8,128)(2,1)S(1)} %bitcast.95), kind=kOutput, calls=%fused_computation.7 | convolution fusion | flops 2097152 | bytes 2164736 | tf_op jit(solution)/shard_map/jeh,jehx->hx/dot_general | solution.py:118
  178.0 33.1 %psum.14 = f32[32,64]{1,0:T(8,128)S(1)} all-reduce(f32[32,64]{1,0:T(8,128)S(1)} %bitcast.110), channel_id=1, replica_groups=mesh['gr'=2,'sp'=8,'tp'=2] {'sp'}, use_global_device_ids=true, to_apply=%region_3.4 | all-reduce | flops 2048 | bytes 16384 | tf_op jit(solution)/shard_map/psum | solution.py:124
  211.7 3.1 %psum.15 = f32[]{:T(128)} all-reduce(f32[]{:T(128)} %multiply_reduce_fusion), channel_id=1, replica_groups=mesh['gr'=2,'sp'=8,'tp'=2] {'tp'}, use_global_device_ids=true, to_apply=%region_5.6 | all-reduce | flops 1 | bytes 8 | tf_op jit(solution)/shard_map/psum | solution.py:126
  (56 shorter events, 5.3 us)
Async XLA Ops:
  7.2 14.1 %all-gather.3.cloned.1.call-start = ((), (), s32[]{:S(2)}) async-start(), calls=%async_computation.1 | async-start | bytes 1572864 | tf_op jit(solution)/shard_map/all_gather | solution.py:80
  21.3 2.6 %copy-start.1 = (bf16[256,2048]{1,0:T(8,128)(2,1)S(1)}, bf16[256,2048]{1,0:T(8,128)(2,1)}, u32[]{:S(2)}) copy-start(bf16[256,2048]{1,0:T(8,128)(2,1)} %all-gather.3.cloned.1.call-done) | copy-start | bytes 3145732
  23.9 5.9 %copy-start.5 = (bf16[2048,1024]{1,0:T(8,128)(2,1)S(1)}, bf16[2048,1024]{1,0:T(8,128)(2,1)}, u32[]{:S(2)}) copy-start(bf16[2048,1024]{1,0:T(8,128)(2,1)} %param.14) | copy-start | bytes 12582916
  31.1 5.1 %collective-permute-start = (bf16[2,3072]{1,0:T(2,128)(2,1)S(1)}, bf16[2,3072]{1,0:T(2,128)(2,1)S(1)}, u32[]{:S(2)}, u32[]{:S(2)}) collective-permute-start(bf16[2,3072]{1,0:T(2,128)(2,1)S(1)} %get-tuple-element.6), channel_id=1, source_target_pairs={{0,2},{2,4},{4,6},{6,8},{8,10},{10,12},{12,14},{1,3},{3,5},{5,7},{... | collective-permute-start | bytes 36872 | tf_op jit(solution)/shard_map/ppermute | solution.py:22
  34.8 5.6 %collective-permute-start.1 = (bf16[2,3072]{1,0:T(2,128)(2,1)S(1)}, bf16[2,3072]{1,0:T(2,128)(2,1)S(1)}, u32[]{:S(2)}, u32[]{:S(2)}) collective-permute-start(bf16[2,3072]{1,0:T(2,128)(2,1)S(1)} %get-tuple-element.7), channel_id=1, source_target_pairs={{2,0},{4,2},{6,4},{8,6},{10,8},{12,10},{14,12},{3,1},{5,3},{7,5},{... | collective-permute-start | bytes 36872 | tf_op jit(solution)/shard_map/ppermute | solution.py:23
  78.8 6.3 %copy-start.4 = (bf16[1,8,128]{2,1,0:T(8,128)(2,1)S(1)}, bf16[1,8,128]{2,1,0:T(8,128)(2,1)}, u32[]{:S(2)}) copy-start(bf16[1,8,128]{2,1,0:T(8,128)(2,1)} %param.20) | copy-start | bytes 6148
  78.9 72.0 %all-to-all-start = ((bf16[8,2,65536]{2,1,0:T(2,128)(2,1)}), bf16[8,2,65536]{2,1,0:T(2,128)(2,1)S(1)}, u32[]{:S(2)}, u32[]{:S(2)}) async-start(bf16[8,2,65536]{2,1,0:T(2,128)(2,1)} %reshape.153), calls=%async_computation | async-start | bytes 4194304 | tf_op jit(solution)/shard_map/all_to_all | solution.py:116
  157.4 53.7 %copy-start.2 = (bf16[1,32,64]{2,1,0:T(8,128)(2,1)S(1)}, bf16[1,32,64]{2,1,0:T(8,128)(2,1)}, u32[]{:S(2)}) copy-start(bf16[1,32,64]{2,1,0:T(8,128)(2,1)} %param.21) | copy-start | bytes 12292
  175.2 40.9 %copy-start = (bf16[2,2,32,8,1024]{4,2,1,0,3:T(8,128)(2,1)}, bf16[2,2,32,8,1024]{4,2,1,0,3:T(8,128)(2,1)S(1)}, u32[]{:S(2)}) copy-start(bf16[2,2,32,8,1024]{4,2,1,0,3:T(8,128)(2,1)S(1)} %copy.84) | copy-start | bytes 6291460
  175.2 40.2 %copy-start.3 = (f32[32,64]{1,0:T(8,128)S(1)}, f32[32,64]{1,0:T(8,128)}, u32[]{:S(2)}) copy-start(f32[32,64]{1,0:T(8,128)} %param.23) | copy-start | bytes 24580
Sparse Core Ops, SparseCore 0:
  9.5 11.7 all-gather.2
where the time goes:
time: 224 us; the launch traced here: 223 us
  blocking collectives  101 us (45%)
  local copies, waits for them, and re-layouts  61.6 us (28%)
  between operations  15.7 us (7%)
  waiting for transfers between devices  14.6 us (7%)
  matrix products  13.5 us (6%)
  starting transfers between devices  10.6 us (5%)
  other arithmetic  5.54 us (2%)
    all_gather x1, blocking collectives, per_device(): all_logs = lax.all_gather(closing, 'sp', axis=0, tiled=True)  65.2 us
    psum x1, blocking collectives, per_device(): read_total = lax.psum(partial_read, 'sp')  33.1 us
    unnamed x20, local copies, waits for them, and re-layouts  20.1 us
    all_to_all x1, local copies, waits for them, and re-layouts, per_device(): lax.all_to_all(local_rows, 'sp', split_axis=3, concat_axis=0, tiled=True)  17.8 us
    convert_element_type x1, local copies, waits for them, and re-layouts, per_device(): states.reshape(span_count, 2, heads_local, N * P_SIZE).astype(jnp.bfloat16)  14.1 us
    all_gather x1, waiting for transfers between devices, per_device(): slab_piece = lax.all_gather(inputs, 'tp', axis=1, tiled=True)  9.82 us
    another operation x2, local copies, waits for them, and re-layouts  6.77 us
    dot_general x1, matrix products, per_device(): x_part = jnp.dot(slab_piece, x_weight, preferred_element_type=jnp.float32)  5.86 us
  transfers between devices with their start and end apart: 4, of which 2 were waited for; matrix products, arithmetic and copies ran while one was open for 2% of the time, Pallas kernels for 0%

commit v1 on v0

--- a/solution.py
+++ b/solution.py
@@ -121,7 +121,11 @@
     picked = lax.dynamic_slice_in_dim(query_c[0], sp_index * columns, columns, 1)
     query_cols = jnp.repeat(picked.astype(jnp.float32), per_group, axis=0)
     partial_read = jnp.einsum("hnp,hn->hp", gathered, query_cols)
-    read_total = lax.psum(partial_read, "sp")
+    read_total = partial_read
+    for hop in (1, 2, 4):
+        read_total = read_total + lax.ppermute(
+            read_total, "sp", [(dev, dev ^ hop) for dev in range(8)]
+        )
     gated_read = read_total * jax.nn.silu(query_gate[0].astype(jnp.float32))
     square_sum = lax.psum(jnp.sum(gated_read * gated_read), "tp")
     mean_square = square_sum / (H * P_SIZE)

time: 224 us -> 203 us (0.906)
  blocking collectives: 101 us -> 68.2 us
  waiting for transfers between devices: 14.6 us -> 26.4 us
    psum x1 -> x0, blocking collectives: 33.1 us -> none  [per_device(): read_total = lax.psum(partial_read, 'sp')]
    ppermute x0 -> x3, waiting for transfers between devices: none -> 11.8 us  [per_device(): lax.ppermute(read_total, 'sp', [(dev, dev ^ hop) for dev in range(8)])]
  transfers between devices with their start and end apart: 4 -> 7, of which waited for: 2 -> 5; matrix products, arithmetic and copies ran while one was open for 2% -> 2% of each run, Pallas kernels for 0% -> 0%
where the time goes in v1:
time: 203 us; the launch traced here: 202 us
  blocking collectives  68.2 us (34%)
  local copies, waits for them, and re-layouts  61.6 us (30%)
  waiting for transfers between devices  26.4 us (13%)
  between operations  15.7 us (8%)
  matrix products  13.5 us (7%)
  starting transfers between devices  10.9 us (5%)
  other arithmetic  5.54 us (3%)
    all_gather x1, blocking collectives, per_device(): all_logs = lax.all_gather(closing, 'sp', axis=0, tiled=True)  65.2 us
    unnamed x20, local copies, waits for them, and re-layouts  20 us
    all_to_all x1, local copies, waits for them, and re-layouts, per_device(): lax.all_to_all(local_rows, 'sp', split_axis=3, concat_axis=0, tiled=True)  17.8 us
    convert_element_type x1, local copies, waits for them, and re-layouts, per_device(): states.reshape(span_count, 2, heads_local, N * P_SIZE).astype(jnp.bfloat16)  14.1 us
    ppermute x3, waiting for transfers between devices, per_device(): lax.ppermute(read_total, 'sp', [(dev, dev ^ hop) for dev in range(8)])  11.8 us
    all_gather x1, waiting for transfers between devices, per_device(): slab_piece = lax.all_gather(inputs, 'tp', axis=1, tiled=True)  9.82 us
    another operation x2, local copies, waits for them, and re-layouts  6.78 us
    dot_general x1, matrix products, per_device(): x_part = jnp.dot(slab_piece, x_weight, preferred_element_type=jnp.float32)  5.86 us
  transfers between devices with their start and end apart: 7, of which 5 were waited for; matrix products, arithmetic and copies ran while one was open for 2% of the time, Pallas kernels for 0%

profile of v1, /device:TPU:0, one launch (start us, length us, event | category | flops | bytes accessed | tf_op | source)
XLA Modules:
  0.0 202.0 jit_solution(18057077288310496597)
XLA Ops:
  8.7 0.8 constant_dynamic-slice_fusion.2
  9.4 1.2 copy.63
  11.5 9.8 %all-gather.3.cloned.1.call-done = bf16[256,2048]{1,0:T(8,128)(2,1)} async-done(((bf16[256,1024]{1,0:T(8,128)(2,1)}), bf16[256,2048]{1,0:T(8,128)(2,1)}) %all-gather.3.cloned.1.call-update) | async-done | bytes 1048592 | tf_op jit(solution)/shard_map/all_gather | solution.py:80
  21.3 1.8 fusion.9
  23.9 5.9 %convolution_convert_fusion = bf16[256,2048]{1,0:T(8,128)(2,1)S(1)} fusion(bf16[256,2048]{1,0:T(8,128)(2,1)S(1)} %copy-done.1, bf16[2048,2048]{1,0:T(8,128)(2,1)} %param.13), kind=kOutput, calls=%fused_computation.3 | convolution fusion | flops 2148007936 | bytes 10485760 | tf_op jit(solution)/shard_map/dot_general | solution.py:81
  29.8 1.3 convolution_convert_fusion.1
  31.1 3.6 %collective-permute-start = (bf16[2,3072]{1,0:T(2,128)(2,1)S(1)}, bf16[2,3072]{1,0:T(2,128)(2,1)S(1)}, u32[]{:S(2)}, u32[]{:S(2)}) collective-permute-start(bf16[2,3072]{1,0:T(2,128)(2,1)S(1)} %get-tuple-element.8), channel_id=1, source_target_pairs={{0,2},{2,4},{4,6},{6,8},{8,10},{10,12},{12,14},{1,3},{3,5},{5,7},{... | collective-permute-start | bytes 36872 | tf_op jit(solution)/shard_map/ppermute | solution.py:22
  34.8 1.3 collective-permute-start.1
  36.3 4.1 %collective-permute-done.1 = bf16[2,3072]{1,0:T(2,128)(2,1)S(1)} collective-permute-done((bf16[2,3072]{1,0:T(2,128)(2,1)S(1)}, bf16[2,3072]{1,0:T(2,128)(2,1)S(1)}, u32[]{:S(2)}, u32[]{:S(2)}) %collective-permute-start.1) | collective-permute-done | bytes 12320 | tf_op jit(solution)/shard_map/ppermute | solution.py:23
  40.9 2.9 %multiply_convert_fusion = bf16[256,3072]{1,0:T(8,128)(2,1)S(1)} fusion(bf16[256,1024]{1,0:T(8,128)(2,1)S(1)} %convolution_convert_fusion.1, bf16[256,2048]{1,0:T(8,128)(2,1)S(1)} %convolution_convert_fusion, bf16[258,3072]{1,0:T(8,128)(2,1)S(1)} %get-tuple-element.7, bf16[258,3072]{1,0:T(8,128)(2,1)S(1)} %get-tuple-element.6, f32[3072]{0:T(1024)S(1)} %bitcast.100, ...), kind=kLoop, calls=%fused_computation.2 | loop fusion | flops 17301504 | bytes 9498624 | tf_op jit(solution)/shard_map/convert_element_type | solution.py:93
  44.0 3.0 %reshape.152 = f32[2,128,32,64]{3,2,1,0:T(8,128)} reshape(f32[256,2048]{1,0:T(8,128)S(1)} %slice_convert_fusion) | data formatting | bytes 4194304 | tf_op jit(solution)/shard_map/convert.7
  47.0 3.8 %copy.62 = f32[2,128,32,64]{1,3,2,0:T(8,128)S(1)} copy(f32[2,128,32,64]{3,2,1,0:T(8,128)} %reshape.152) | data formatting | bytes 4194304 | tf_op jit(solution)/shard_map/convert.7
  51.6 2.0 %convert_bitcast_fusion = bf16[2,2,32,128,64]{3,4,1,2,0:T(8,128)(2,1)} fusion(bf16[2,128,32,128,1]{3,1,4,2,0:T(8,128)(2,1)S(1)} %bitcast.91, f32[2,128,32,2]{1,3,2,0:T(2,128)S(1)} %copy.68, f32[2,128,32,64]{1,3,2,0:T(8,128)S(1)} %copy.62), kind=kOutput, calls=%fused_computation.9 | convolution fusion | flops 270532608 | bytes 6356992 | tf_op jit(solution)/shard_map/kseh,kshn,kshp->kehnp/dot_general | solution.py:34
  53.6 14.1 %copy.82 = bf16[2,2,32,128,64]{2,1,0,4,3:T(2,128)(2,1)} copy(bf16[2,2,32,128,64]{3,4,1,2,0:T(8,128)(2,1)} %convert_bitcast_fusion) | data formatting | bytes 4194304 | tf_op jit(solution)/shard_map/convert_element_type | solution.py:113
  67.7 11.2 %reshape.153 = bf16[8,2,65536]{2,1,0:T(2,128)(2,1)} reshape(bf16[8192,2,2,32]{3,2,1,0:T(2,128)(2,1)} %bitcast.89) | data formatting | bytes 4194304
  78.9 5.6 %all-to-all-start = ((bf16[8,2,65536]{2,1,0:T(2,128)(2,1)}), bf16[8,2,65536]{2,1,0:T(2,128)(2,1)S(1)}, u32[]{:S(2)}, u32[]{:S(2)}) async-start(bf16[8,2,65536]{2,1,0:T(2,128)(2,1)} %reshape.153), calls=%async_computation | async-start | bytes 4194304 | tf_op jit(solution)/shard_map/all_to_all | solution.py:116
  85.3 65.2 %all-gather = f32[16,1,2,32]{3,2,1,0:T(2,128)S(1)} all-gather(f32[2,1,2,32]{3,2,1,0:T(2,128)S(1)} %get-tuple-element.10), channel_id=2, replica_groups=mesh['gr'=2,'sp'=8,'tp'=2] {'sp'}, dimensions={0}, use_global_device_ids=true | all-gather | bytes 4608 | tf_op jit(solution)/shard_map/all_gather | solution.py:114
  150.8 6.5 %reshape.154 = bf16[8192,2,2,32]{3,2,1,0:T(2,128)(2,1)} reshape(bf16[8,2,65536]{2,1,0:T(2,128)(2,1)S(1)} %all-to-all-done) | data formatting | bytes 4194304
  157.4 17.8 %copy.84 = bf16[2,2,32,8,1024]{4,2,1,0,3:T(8,128)(2,1)S(1)} copy(bf16[2,2,32,8,1024]{2,1,0,4,3:T(2,128)(2,1)} %bitcast.90) | data formatting | bytes 4194304 | tf_op jit(solution)/shard_map/all_to_all | solution.py:116
  175.2 2.4 %fusion.2 = bf16[32,1,1024,1]{2,1,3,0:T(2,128)(2,1)S(1)} fusion(bf16[16,2,32,1]{0,3,1,2:T(2,128)(2,1)S(1)} %copy.75, bf16[16,2,32,1024]{3,2,1,0:T(8,128)(2,1)S(1)} %bitcast.92), kind=kOutput, calls=%fused_computation.7 | convolution fusion | flops 2097152 | bytes 2164736 | tf_op jit(solution)/shard_map/jeh,jehx->hx/dot_general | solution.py:118
  178.1 3.7 %collective-permute-done.2 = f32[32,64]{1,0:T(8,128)S(1)} collective-permute-done((f32[32,64]{1,0:T(8,128)S(1)}, f32[32,64]{1,0:T(8,128)S(1)}, u32[]{:S(2)}, u32[]{:S(2)}) %collective-permute-start.2) | collective-permute-done | bytes 8224 | tf_op jit(solution)/shard_map/ppermute | solution.py:126
  182.1 3.5 %collective-permute-done.3 = f32[32,64]{1,0:T(8,128)S(1)} collective-permute-done((f32[32,64]{1,0:T(8,128)S(1)}, f32[32,64]{1,0:T(8,128)S(1)}, u32[]{:S(2)}, u32[]{:S(2)}) %collective-permute-start.3) | collective-permute-done | bytes 8224 | tf_op jit(solution)/shard_map/ppermute | solution.py:126
  185.5 4.6 %collective-permute-done.4 = f32[32,64]{1,0:T(8,128)S(1)} collective-permute-done((f32[32,64]{1,0:T(8,128)S(1)}, f32[32,64]{1,0:T(8,128)S(1)}, u32[]{:S(2)}, u32[]{:S(2)}) %collective-permute-start.4) | collective-permute-done | bytes 8224 | tf_op jit(solution)/shard_map/ppermute | solution.py:126
  190.8 3.1 %psum.7 = f32[]{:T(128)} all-reduce(f32[]{:T(128)} %get-tuple-element.2), channel_id=1, replica_groups=mesh['gr'=2,'sp'=8,'tp'=2] {'tp'}, use_global_device_ids=true, to_apply=%region_4.5 | all-reduce | flops 1 | bytes 8 | tf_op jit(solution)/shard_map/psum | solution.py:130
  (63 shorter events, 7.1 us)
Async XLA Ops:
  7.2 14.1 %all-gather.3.cloned.1.call-start = ((), (), s32[]{:S(2)}) async-start(), calls=%async_computation.1 | async-start | bytes 1572864 | tf_op jit(solution)/shard_map/all_gather | solution.py:80
  21.3 2.6 %copy-start.1 = (bf16[256,2048]{1,0:T(8,128)(2,1)S(1)}, bf16[256,2048]{1,0:T(8,128)(2,1)}, u32[]{:S(2)}) copy-start(bf16[256,2048]{1,0:T(8,128)(2,1)} %all-gather.3.cloned.1.call-done) | copy-start | bytes 3145732
  23.9 5.9 %copy-start.5 = (bf16[2048,1024]{1,0:T(8,128)(2,1)S(1)}, bf16[2048,1024]{1,0:T(8,128)(2,1)}, u32[]{:S(2)}) copy-start(bf16[2048,1024]{1,0:T(8,128)(2,1)} %param.14) | copy-start | bytes 12582916
  31.1 5.1 %collective-permute-start = (bf16[2,3072]{1,0:T(2,128)(2,1)S(1)}, bf16[2,3072]{1,0:T(2,128)(2,1)S(1)}, u32[]{:S(2)}, u32[]{:S(2)}) collective-permute-start(bf16[2,3072]{1,0:T(2,128)(2,1)S(1)} %get-tuple-element.8), channel_id=1, source_target_pairs={{0,2},{2,4},{4,6},{6,8},{8,10},{10,12},{12,14},{1,3},{3,5},{5,7},{... | collective-permute-start | bytes 36872 | tf_op jit(solution)/shard_map/ppermute | solution.py:22
  34.8 5.6 %collective-permute-start.1 = (bf16[2,3072]{1,0:T(2,128)(2,1)S(1)}, bf16[2,3072]{1,0:T(2,128)(2,1)S(1)}, u32[]{:S(2)}, u32[]{:S(2)}) collective-permute-start(bf16[2,3072]{1,0:T(2,128)(2,1)S(1)} %get-tuple-element.9), channel_id=1, source_target_pairs={{2,0},{4,2},{6,4},{8,6},{10,8},{12,10},{14,12},{3,1},{5,3},{7,5},{... | collective-permute-start | bytes 36872 | tf_op jit(solution)/shard_map/ppermute | solution.py:23
  78.9 6.3 %copy-start.4 = (bf16[1,8,128]{2,1,0:T(8,128)(2,1)S(1)}, bf16[1,8,128]{2,1,0:T(8,128)(2,1)}, u32[]{:S(2)}) copy-start(bf16[1,8,128]{2,1,0:T(8,128)(2,1)} %param.20) | copy-start | bytes 6148
  78.9 72.0 %all-to-all-start = ((bf16[8,2,65536]{2,1,0:T(2,128)(2,1)}), bf16[8,2,65536]{2,1,0:T(2,128)(2,1)S(1)}, u32[]{:S(2)}, u32[]{:S(2)}) async-start(bf16[8,2,65536]{2,1,0:T(2,128)(2,1)} %reshape.153), calls=%async_computation | async-start | bytes 4194304 | tf_op jit(solution)/shard_map/all_to_all | solution.py:116
  175.2 20.0 %copy-start = (bf16[2,2,32,8,1024]{4,2,1,0,3:T(8,128)(2,1)}, bf16[2,2,32,8,1024]{4,2,1,0,3:T(8,128)(2,1)S(1)}, u32[]{:S(2)}) copy-start(bf16[2,2,32,8,1024]{4,2,1,0,3:T(8,128)(2,1)S(1)} %copy.84) | copy-start | bytes 6291460
  175.2 15.0 %copy-start.3 = (bf16[1,32,64]{2,1,0:T(8,128)(2,1)S(1)}, bf16[1,32,64]{2,1,0:T(8,128)(2,1)}, u32[]{:S(2)}) copy-start(bf16[1,32,64]{2,1,0:T(8,128)(2,1)} %param.21) | copy-start | bytes 12292
  175.2 19.4 %copy-start.2 = (f32[32,64]{1,0:T(8,128)S(1)}, f32[32,64]{1,0:T(8,128)}, u32[]{:S(2)}) copy-start(f32[32,64]{1,0:T(8,128)} %param.23) | copy-start | bytes 24580
  178.0 3.8 %collective-permute-start.2 = (f32[32,64]{1,0:T(8,128)S(1)}, f32[32,64]{1,0:T(8,128)S(1)}, u32[]{:S(2)}, u32[]{:S(2)}) collective-permute-start(f32[32,64]{1,0:T(8,128)S(1)} %bitcast.106), channel_id=1, source_target_pairs={{0,2},{2,0},{4,6},{6,4},{8,10},{10,8},{12,14},{14,12},{1,3},{3,1},... | collective-permute-start | bytes 24584 | tf_op jit(solution)/shard_map/ppermute | solution.py:126
  181.8 3.7 %collective-permute-start.3 = (f32[32,64]{1,0:T(8,128)S(1)}, f32[32,64]{1,0:T(8,128)S(1)}, u32[]{:S(2)}, u32[]{:S(2)}) collective-permute-start(f32[32,64]{1,0:T(8,128)S(1)} %add.73), channel_id=1, source_target_pairs={{0,4},{2,6},{4,0},{6,2},{8,12},{10,14},{12,8},{14,10},{1,5},{3,7},... | collective-permute-start | bytes 24584 | tf_op jit(solution)/shard_map/ppermute | solution.py:126
  185.5 4.6 %collective-permute-start.4 = (f32[32,64]{1,0:T(8,128)S(1)}, f32[32,64]{1,0:T(8,128)S(1)}, u32[]{:S(2)}, u32[]{:S(2)}) collective-permute-start(f32[32,64]{1,0:T(8,128)S(1)} %add.74), channel_id=1, source_target_pairs={{0,8},{2,10},{4,12},{6,14},{8,0},{10,2},{12,4},{14,6},{1,9},{3,11}... | collective-permute-start | bytes 24584 | tf_op jit(solution)/shard_map/ppermute | solution.py:126
Sparse Core Ops, SparseCore 0:
  9.5 11.7 all-gather.2
